TPU v7x, 32 devices: a whole 2x2x4 slice. The times are simulated.
32 devices in a mesh: sp: 4 (over y, x), tp: 8 (over z, core).
Axes of the slice: x: 2, y: 2, z: 4, core: 2. Of those that a mesh axis runs over, the one named last changes fastest.
Arguments:
- tokens: bfloat16 [2048, 2048], P(('sp', 'tp')), may hold values from -6 to 6
- query_vectors: bfloat16 [2048, 2048], P('sp', 'tp'), may hold values from -8 to 8
- key_vectors: bfloat16 [2048, 2048], P('sp', 'tp'), may hold values from -8 to 8
- value_vectors: bfloat16 [2048, 2048], P('sp', 'tp'), may hold values from -24 to 24
- cum_gate: float32 [2048, 32], P('sp', 'tp'), may hold values from -260 to 0, as said below
- out_weight: bfloat16 [2048, 2048], P('tp'), may hold values from -0.125 to 0.125
- norm_gain: float32 [2048], replicated, may hold values from 0.1 to 1.9
- gate_weight: bfloat16 [4, 2048, 7168], P('sp', None, 'tp'), may hold values from -0.125 to 0.125
- up_weight: bfloat16 [4, 2048, 7168], P('sp', None, 'tp'), may hold values from -0.125 to 0.125
- down_weight: bfloat16 [4, 7168, 2048], P('sp', 'tp'), may hold values from -0.0625 to 0.0625
- expert_ids: int32 [2048, 2], P(('sp', 'tp')), may hold values from 0 to 3, all different within a row; in each aligned block of 64 rows (0 to 63, 64 to 127, ...) at most 48 rows name the same one
- route_weights: float32 [2048, 2], P(('sp', 'tp')), may hold values from 0.2 to 1
Outputs:
- layer_output: bfloat16 [2048, 2048], P(('sp', 'tp'))
Inputs may be any that keep to these rules, and one draw needn't show every extreme that they name: `cum_gate`: along the positions each head's values never rise. `expert_ids`: within the rows of one device no expert is named by more than 48 rows, and in some devices' rows one expert is named by exactly 48; a row names 2 different experts.
All inputs are finite; a program needn't handle non-finite values.
Results may differ from a plain program's by a relative error of at most 0.014.
Values may be sent and summed in bfloat16 or wider, within the bound.
A program may use at most 128 MiB of HBM per device.

v0:
```python
import math
import jax
import jax.numpy as jnp
from jax import lax
from jax.sharding import PartitionSpec as P

NEG_LARGE = -1e30


def shards(
    tokens,
    query_vectors,
    key_vectors,
    value_vectors,
    cum_gate,
    out_weight,
    norm_gain,
    gate_weight,
    up_weight,
    down_weight,
    expert_ids,
    route_weights,
):
    sp_count = lax.axis_size("sp")
    seg_rows = query_vectors.shape[0]
    heads_here = cum_gate.shape[1]
    head_width = query_vectors.shape[1] // heads_here
    score_scale = head_width ** (-0.5)
    offset = lax.axis_index("sp") * seg_rows
    last_query = offset + seg_rows - 1
    query_pos = offset + jnp.arange(seg_rows, dtype=jnp.int32)
    query_heads = query_vectors.reshape(seg_rows, heads_here, head_width)
    query_gate = cum_gate.T
    gate_rows = lax.all_gather(cum_gate, "sp", axis=0, tiled=True)

    def attend_block(carried, key_block, value_block, block_start):
        running_peak, running_total, accumulated = carried
        row_count = key_block.shape[0]
        key_heads = key_block.reshape(row_count, heads_here, head_width)
        value_heads = value_block.reshape(row_count, heads_here, head_width)
        key_gate = lax.dynamic_slice_in_dim(gate_rows, block_start, row_count, 0).T
        scores = (
            jnp.einsum("qhd,khd->hqk", query_heads, key_heads, preferred_element_type=jnp.float32)
            * score_scale
        )
        scores = scores + query_gate[:, :, None] - key_gate[:, None, :]
        key_pos = block_start + jnp.arange(row_count, dtype=jnp.int32)
        visible = (key_pos[None, :] <= query_pos[:, None])[None]
        scores = jnp.where(visible, scores, NEG_LARGE)
        new_peak = jnp.maximum(running_peak, jnp.max(scores, axis=2))
        exponent = jnp.where(visible, jnp.exp(scores - new_peak[:, :, None]), 0.0)
        rescale = jnp.exp(running_peak - new_peak)
        running_total = running_total * rescale + jnp.sum(exponent, axis=2)
        weighted = jnp.einsum(
            "hqk,khd->hqd",
            exponent.astype(jnp.bfloat16),
            value_heads,
            preferred_element_type=jnp.float32,
        )
        accumulated = accumulated * rescale[:, :, None] + weighted
        return (new_peak, running_total, accumulated)

    start_state = (
        jnp.full((heads_here, seg_rows), NEG_LARGE, jnp.float32),
        jnp.zeros((heads_here, seg_rows), jnp.float32),
        jnp.zeros((heads_here, seg_rows, head_width), jnp.float32),
    )
    carried = start_state
    key_piece = lax.all_gather(key_vectors, "sp", axis=0, tiled=True)
    value_piece = lax.all_gather(value_vectors, "sp", axis=0, tiled=True)
    row_count = key_piece.shape[0]
    block_rows = math.gcd(row_count, 1024)
    block_count = row_count // block_rows
    key_stack = key_piece.reshape(block_count, block_rows, key_piece.shape[1])
    value_stack = value_piece.reshape(block_count, block_rows, value_piece.shape[1])

    def step_block(state, inputs):
        key_block, value_block, block_index = inputs
        block_start = block_index * block_rows

        def take_block(inner):
            return attend_block(inner, key_block, value_block, block_start)

        def skip_block(inner):
            return inner

        return (lax.cond(block_start <= last_query, take_block, skip_block, state), None)

    carried, _ = lax.scan(
        step_block, carried, (key_stack, value_stack, jnp.arange(block_count, dtype=jnp.int32))
    )
    final_peak, final_total, accumulated = carried
    attended = (accumulated / final_total[:, :, None]).astype(jnp.bfloat16)
    attended = attended.transpose(1, 0, 2).reshape(seg_rows, heads_here * head_width)
    tok_dev = tokens.shape[0]
    model_width = tokens.shape[1]
    token_rows = lax.all_to_all(attended, "tp", split_axis=0, concat_axis=1, tiled=True)
    projected = jnp.dot(
        token_rows,
        lax.all_gather(out_weight, "tp", axis=0, tiled=True),
        preferred_element_type=jnp.float32,
    )
    stream_wide = (tokens.astype(jnp.float32) + projected).astype(jnp.bfloat16).astype(jnp.float32)
    inverse = lax.rsqrt(jnp.mean(stream_wide * stream_wide, axis=1, keepdims=True) + 1e-05)
    normed = (stream_wide * inverse * norm_gain[None, :]).astype(jnp.bfloat16)
    n_experts = gate_weight.shape[0] * sp_count
    top_count = expert_ids.shape[1]
    capacity = max(2, 3 * tok_dev * top_count // (2 * n_experts))
    flat_ids = expert_ids.reshape(-1)
    hits = (flat_ids[:, None] == jnp.arange(n_experts, dtype=jnp.int32)[None, :]).astype(jnp.int32)
    earlier = jnp.cumsum(hits, axis=0) - hits
    slot_index = flat_ids * capacity + jnp.sum(earlier * hits, axis=1)
    placement_map = (
        jnp.arange(n_experts * capacity, dtype=jnp.int32)[:, None] == slot_index[None, :]
    ).astype(jnp.bfloat16)
    repeated = jnp.repeat(normed, top_count, axis=0)
    dispatch = jnp.dot(placement_map, repeated, preferred_element_type=jnp.float32).astype(
        jnp.bfloat16
    )
    dispatch = dispatch.reshape(n_experts, capacity, model_width)
    arrived = lax.all_to_all(dispatch, "sp", split_axis=0, concat_axis=0, tiled=True)
    row_block = arrived.reshape(-1, model_width)
    rows_in = lax.all_gather(row_block, "tp", axis=0, tiled=True)
    gate_value = jnp.dot(rows_in, gate_weight[0], preferred_element_type=jnp.float32)
    up_value = jnp.dot(rows_in, up_weight[0], preferred_element_type=jnp.float32)
    hidden = (jax.nn.silu(gate_value) * up_value).astype(jnp.bfloat16)
    summed = lax.psum_scatter(
        jnp.dot(hidden, down_weight[0], preferred_element_type=jnp.float32).astype(jnp.bfloat16),
        "tp",
        scatter_dimension=0,
        tiled=True,
    )
    returned = summed.reshape(arrived.shape)
    back = lax.all_to_all(returned, "sp", split_axis=0, concat_axis=0, tiled=True)
    flat_back = back.reshape(n_experts * capacity, model_width)
    picked = flat_back[slot_index].astype(jnp.float32).reshape(tok_dev, top_count, model_width)
    mixture = jnp.sum(picked * route_weights[:, :, None], axis=1)
    return (stream_wide + mixture).astype(jnp.bfloat16)


def solution(mesh):
    in_specs = (
        P(("sp", "tp"), None),
        P("sp", "tp"),
        P("sp", "tp"),
        P("sp", "tp"),
        P("sp", "tp"),
        P("tp", None),
        P(),
        P("sp", None, "tp"),
        P("sp", None, "tp"),
        P("sp", "tp", None),
        P(("sp", "tp"), None),
        P(("sp", "tp"), None),
    )
    out_specs = P(("sp", "tp"), None)
    return jax.shard_map(shards, mesh=mesh, in_specs=in_specs, out_specs=out_specs, check_vma=False)
```

profile of v0, /device:TPU:0, one launch (start us, length us, event | category | flops | bytes accessed | tf_op | source)
XLA Modules:
  0.0 362.4 jit_solution(4247297287543457111)
XLA Ops:
  8.7 1.1 copy.27
  10.8 9.8 %all_gather.16 = f32[2048,4]{0,1:T(4,128)S(1)} all-gather(f32[512,4]{0,1:T(4,128)} %param.20), channel_id=1, replica_groups=mesh['sp'=4,'tp'=8] {'sp'}, dimensions={0}, use_global_device_ids=true | all-gather | bytes 40960 | tf_op jit(solution)/shard_map/all_gather | solution.py:34
  20.6 17.9 %all-gather.5.cloned.1.call-done = bf16[2048,256]{1,0:T(8,128)(2,1)} async-done(((bf16[512,256]{1,0:T(8,128)(2,1)}), bf16[2048,256]{1,0:T(8,128)(2,1)}) %all-gather.5.cloned.1.call-update) | async-done | bytes 1048592 | tf_op jit(solution)/shard_map/all_gather | solution.py:69
  38.4 1.5 copy.28
  39.9 26.9 %all-gather.7.cloned.1.call-done = bf16[2048,256]{1,0:T(8,128)(2,1)} async-done(((bf16[512,256]{1,0:T(8,128)(2,1)}), bf16[2048,256]{1,0:T(8,128)(2,1)}) %all-gather.7.cloned.1.call-update) | async-done | bytes 1048592 | tf_op jit(solution)/shard_map/all_gather | solution.py:70
  66.8 1.5 copy.29
  68.4 12.0 %while.15 = (s32[]{:T(128)}, f32[4,512]{1,0:T(4,128)S(1)}, f32[4,512]{1,0:T(4,128)S(1)}, f32[4,512,64]{1,2,0:T(8,128)S(1)}, s32[2]{0:T(128)S(1)}, /*index=5*/s32...) while((s32[]{:T(128)}, f32[4,512]{1,0:T(4,128)S(1)}, ...), condition=%wide.region_5.6_spmd.clone, body=%wide.region_0.5_spmd.clone.sunk | while | flops 577508864 | bytes 31973748 | solution.py:89
  69.8 9.2 %conditional.3 = ((f32[4,512]{1,0:T(4,128)S(1)}, f32[4,512]{1,0:T(4,128)S(1)}, f32[4,512,64]{1,2,0:T(8,128)S(1)})) conditional(s32[]{:T(128)} %convert_element_type.83, (f32[4,512]{1,0:T(4,128)S(1)}, f32[4,512]{1,0:T(4,128)S(1)}, f32[4,512,64]{1,2,0:T(8,128)S(1)}) %tuple.42, (s32[]{:T(128)}, s32[]{:T(128)}, bf16[2,1024,256]{1,2,0:T(8,128)(2,1)S(1)}, ...), branch_computations={%region_1.1_spmd, %region_2.4_spmd} | conditional | flops 577508864 | bytes 31971410 | solution.py:87
  70.4 2.5 fusion.4
  72.9 2.9 fusion.3
  75.8 3.2 fusion.8
  80.8 1.0 copy.30
  81.8 4.6 %all-to-all-start = ((bf16[8,64,256]{2,1,0:T(8,128)(2,1)}), bf16[8,64,256]{2,1,0:T(8,128)(2,1)S(1)}, u32[]{:S(2)}, u32[]{:S(2)}) async-start(bf16[8,64,256]{2,1,0:T(8,128)(2,1)} %copy.30), calls=%async_computation | async-start | bytes 524288 | tf_op jit(solution)/shard_map/all_to_all | solution.py:97
  86.9 15.4 %all-to-all-done = bf16[8,64,256]{2,1,0:T(8,128)(2,1)S(1)} async-done(((bf16[8,64,256]{2,1,0:T(8,128)(2,1)}), bf16[8,64,256]{2,1,0:T(8,128)(2,1)S(1)}, u32[]{:S(2)}, u32[]{:S(2)}) %all-to-all-start) | async-done | bytes 262176 | tf_op jit(solution)/shard_map/all_to_all | solution.py:97
  102.3 53.7 %all-gather.9.cloned.1.call-done = bf16[2048,2048]{1,0:T(8,128)(2,1)} async-done(((bf16[256,2048]{1,0:T(8,128)(2,1)}), bf16[2048,2048]{1,0:T(8,128)(2,1)}) %all-gather.9.cloned.1.call-update) | async-done | bytes 8388624 | tf_op jit(solution)/shard_map/all_gather | solution.py:100
  156.0 5.1 %multiply_reduce_fusion.1 = (f32[64]{0:T(128)S(1)}, f32[64,2048]{1,0:T(8,128)S(1)}) fusion(bf16[64,2048]{1,0:T(8,128)(2,1)S(1)} %bitcast.63, bf16[2048,2048]{1,0:T(8,128)(2,1)} %all-gather.9.cloned.1.call-done, bf16[64,2048]{1,0:T(8,128)(2,1)S(1)} %copy-done.1), kind=kOutput, calls=%fused_computation.35 | convolution fusion | flops 537657280 | bytes 9437440 | tf_op jit(solution)/shard_map/dot_general | solution.py:98
  162.1 15.3 %all_to_all.29 = bf16[4,48,2048]{2,1,0:T(8,128)(2,1)} all-to-all(bf16[4,48,2048]{2,1,0:T(8,128)(2,1)S(1)} %bitcast.62), channel_id=1, replica_groups=mesh['sp'=4,'tp'=8] {'sp'}, dimensions={0} | all-to-all | bytes 1572864 | tf_op jit(solution)/shard_map/all_to_all | solution.py:121
  177.5 61.7 %all-gather.11.cloned.1.call-done = bf16[1536,2048]{1,0:T(8,128)(2,1)} async-done(((bf16[192,2048]{1,0:T(8,128)(2,1)}), bf16[1536,2048]{1,0:T(8,128)(2,1)}) %all-gather.11.cloned.1.call-update) | async-done | bytes 6291472 | tf_op jit(solution)/shard_map/all_gather | solution.py:123
  239.3 11.4 %fusion.18 = f32[1536,896]{1,0:T(8,128)} fusion(bf16[1536,2048]{1,0:T(8,128)(2,1)} %all-gather.11.cloned.1.call-done, bf16[1,2048,896]{2,1,0:T(8,128)(2,1)} %param.23), kind=kOutput, calls=%fused_computation.25 | convolution fusion | flops 5637144576 | bytes 15466496 | tf_op jit(solution)/shard_map/dot_general | solution.py:124
  250.6 20.1 %convolution_convert_fusion = bf16[1536,2048]{1,0:T(8,128)(2,1)} fusion(bf16[1,896,2048]{2,1,0:T(8,128)(2,1)} %param.25, f32[1536,896]{1,0:T(8,128)} %fusion.18, bf16[1536,2048]{1,0:T(8,128)(2,1)} %all-gather.11.cloned.1.call-done, bf16[1,2048,896]{2,1,0:T(8,128)(2,1)} %param.24), kind=kOutput, calls=%fused_computation.21 | convolution fusion | flops 11285692416 | bytes 25427968 | tf_op jit(solution)/shard_map/dot_general | solution.py:128
  270.7 68.5 %reduce-scatter.2.cloned.1.call-done = bf16[192,2048]{1,0:T(8,128)(2,1)} async-done(((bf16[1536,2048]{1,0:T(8,128)(2,1)}), bf16[192,2048]{1,0:T(8,128)(2,1)}) %reduce-scatter.2.cloned.1.call-update) | async-done | bytes 786448 | tf_op jit(solution)/shard_map/reduce_scatter | solution.py:127
  339.2 3.7 %all-to-all-start.2 = ((bf16[4,48,2048]{2,1,0:T(8,128)(2,1)}), bf16[4,48,2048]{2,1,0:T(8,128)(2,1)S(1)}, u32[]{:S(2)}, u32[]{:S(2)}) async-start(bf16[4,48,2048]{2,1,0:T(8,128)(2,1)} %bitcast.67), calls=%async_computation.3 | async-start | bytes 1572864 | tf_op jit(solution)/shard_map/all_to_all | solution.py:134
  343.3 8.7 %all-to-all-done.2 = bf16[4,48,2048]{2,1,0:T(8,128)(2,1)S(1)} async-done(((bf16[4,48,2048]{2,1,0:T(8,128)(2,1)}), bf16[4,48,2048]{2,1,0:T(8,128)(2,1)S(1)}, u32[]{:S(2)}, u32[]{:S(2)}) %all-to-all-start.2) | async-done | bytes 786464 | tf_op jit(solution)/shard_map/all_to_all | solution.py:134
  353.6 1.5 multiply_reduce_fusion
  (60 shorter events, 9.6 us)
Async XLA Ops:
  6.5 61.8 %copy-start = (f32[512,4]{0,1:T(4,128)S(1)}, f32[512,4]{0,1:T(4,128)}, u32[]{:S(2)}) copy-start(f32[512,4]{0,1:T(4,128)} %param.20) | copy-start | bytes 24580
  6.5 31.9 %all-gather.5.cloned.1.call-start = ((), (), s32[]{:S(2)}) async-start(), calls=%async_computation.4 | async-start | bytes 1310720 | tf_op jit(solution)/shard_map/all_gather | solution.py:69
  7.3 59.5 %all-gather.7.cloned.1.call-start = ((), (), s32[]{:S(2)}) async-start(), calls=%async_computation.5 | async-start | bytes 1310720 | tf_op jit(solution)/shard_map/all_gather | solution.py:70
  8.0 148.0 %all-gather.9.cloned.1.call-start = ((), (), s32[]{:S(2)}) async-start(), calls=%async_computation.6 | async-start | bytes 9437184 | tf_op jit(solution)/shard_map/all_gather | solution.py:100
  68.4 87.6 %copy-start.1 = (bf16[64,2048]{1,0:T(8,128)(2,1)S(1)}, bf16[64,2048]{1,0:T(8,128)(2,1)}, u32[]{:S(2)}) copy-start(bf16[64,2048]{1,0:T(8,128)(2,1)} %param.16) | copy-start | bytes 786436
  81.8 20.5 %all-to-all-start = ((bf16[8,64,256]{2,1,0:T(8,128)(2,1)}), bf16[8,64,256]{2,1,0:T(8,128)(2,1)S(1)}, u32[]{:S(2)}, u32[]{:S(2)}) async-start(bf16[8,64,256]{2,1,0:T(8,128)(2,1)} %copy.30), calls=%async_computation | async-start | bytes 524288 | tf_op jit(solution)/shard_map/all_to_all | solution.py:97
  86.4 152.9 %all-gather.11.cloned.1.call-start = ((), (), s32[]{:S(2)}) async-start(), calls=%async_computation.7 | async-start | bytes 7077888 | tf_op jit(solution)/shard_map/all_gather | solution.py:123
  156.0 5.1 %copy-start.2 = (f32[2048]{0:T(1024)S(1)}, f32[2048]{0:T(1024)}, u32[]{:S(2)}) copy-start(f32[2048]{0:T(1024)} %param.22) | copy-start | bytes 24580
  177.5 161.8 %reduce-scatter.2.cloned.1.call-start = ((), (), s32[]{:S(2)}) async-start(), calls=%async_computation.8 | async-start | bytes 7077888 | tf_op jit(solution)/shard_map/reduce_scatter | solution.py:127
  270.7 72.2 %copy-start.3 = (s32[64,2]{0,1:T(2,128)S(1)}, s32[64,2]{0,1:T(2,128)}, u32[]{:S(2)}) copy-start(s32[64,2]{0,1:T(2,128)} %param.26) | copy-start | bytes 1540
  270.7 72.5 %copy-start.4 = (f32[64,2]{0,1:T(2,128)S(1)}, f32[64,2]{0,1:T(2,128)}, u32[]{:S(2)}) copy-start(f32[64,2]{0,1:T(2,128)} %param.27) | copy-start | bytes 1540
  339.2 12.8 %all-to-all-start.2 = ((bf16[4,48,2048]{2,1,0:T(8,128)(2,1)}), bf16[4,48,2048]{2,1,0:T(8,128)(2,1)S(1)}, u32[]{:S(2)}, u32[]{:S(2)}) async-start(bf16[4,48,2048]{2,1,0:T(8,128)(2,1)} %bitcast.67), calls=%async_computation.3 | async-start | bytes 1572864 | tf_op jit(solution)/shard_map/all_to_all | solution.py:134
Sparse Core Ops, SparseCore 0:
  9.2 29.2 all-gather.4
  40.3 26.4 all-gather.6
  68.4 87.5 all-gather.8
  177.6 61.6 all-gather.10
  270.8 68.3 reduce-scatter.1
where the time goes:
time: 363 us; the launch traced here: 362 us
  waiting for transfers between devices  255 us (70%)
  matrix products  42.6 us (12%)
  blocking collectives  25.1 us (7%)
  between operations  13.4 us (4%)
  local copies, waits for them, and re-layouts  10.3 us (3%)
  starting transfers between devices  8.43 us (2%)
  other arithmetic  6.2 us (2%)
    reduce_scatter x1, waiting for transfers between devices, shards(): lax.psum_scatter(jnp.dot(hidden, down_weight[0], preferred_element_type=j...  68.5 us
    all_gather x1, waiting for transfers between devices, shards(): rows_in = lax.all_gather(row_block, 'tp', axis=0, tiled=True)  61.7 us
    all_gather x1, waiting for transfers between devices, shards(): lax.all_gather(out_weight, 'tp', axis=0, tiled=True)  53.7 us
    all_gather x1, waiting for transfers between devices, shards(): value_piece = lax.all_gather(value_vectors, 'sp', axis=0, tiled=True)  26.9 us
    dot_general x1, matrix products, shards(): jnp.dot(hidden, down_weight[0], preferred_element_type=jnp.float32)  20.1 us
    all_gather x1, waiting for transfers between devices, shards(): key_piece = lax.all_gather(key_vectors, 'sp', axis=0, tiled=True)  17.9 us
    all_to_all x1, waiting for transfers between devices, shards(): lax.all_to_all(attended, 'tp', split_axis=0, concat_axis=1, tiled=True)  15.4 us
    all_to_all x1, blocking collectives, shards(): lax.all_to_all(dispatch, 'sp', split_axis=0, concat_axis=0, tiled=True)  15.3 us
  transfers between devices with their start and end apart: 7, of which 7 were waited for; matrix products, arithmetic and copies ran while one was open for 5% of the time, Pallas kernels for 0%

commit v1 on v0

--- a/solution.py
+++ b/solution.py
@@ -5,6 +5,18 @@
 from jax.sharding import PartitionSpec as P
 
 NEG_LARGE = -1e30
+
+
+def collect(array, axis, dim):
+    ways, here = (lax.axis_size(axis), lax.axis_index(axis))
+    grown, reach = (array, 1)
+    while reach < ways:
+        theirs = lax.ppermute(grown, axis, [(d, d ^ reach) for d in range(ways)])
+        mine_first = jnp.concatenate([grown, theirs], axis=dim)
+        theirs_first = jnp.concatenate([theirs, grown], axis=dim)
+        grown = jnp.where(here & reach == 0, mine_first, theirs_first)
+        reach = 2 * reach
+    return grown
 
 
 def shards(
@@ -96,9 +108,7 @@
     model_width = tokens.shape[1]
     token_rows = lax.all_to_all(attended, "tp", split_axis=0, concat_axis=1, tiled=True)
     projected = jnp.dot(
-        token_rows,
-        lax.all_gather(out_weight, "tp", axis=0, tiled=True),
-        preferred_element_type=jnp.float32,
+        token_rows, collect(out_weight, "tp", 0), preferred_element_type=jnp.float32
     )
     stream_wide = (tokens.astype(jnp.float32) + projected).astype(jnp.bfloat16).astype(jnp.float32)
     inverse = lax.rsqrt(jnp.mean(stream_wide * stream_wide, axis=1, keepdims=True) + 1e-05)

time: 363 us -> 466 us (1.28)
  waiting for transfers between devices: 255 us -> 347 us
  other arithmetic: 6.2 us -> 13.7 us
  starting transfers between devices: 8.43 us -> 14.8 us
    all_to_all x1, waiting for transfers between devices: 15.4 us -> 112 us  [shards(): lax.all_to_all(attended, 'tp', split_axis=0, concat_axis=1, tiled=True)]
    all_gather x1 -> x0, waiting for transfers between devices: 53.7 us -> none  [shards(): lax.all_gather(out_weight, 'tp', axis=0, tiled=True)]
    ppermute x0 -> x3, waiting for transfers between devices: none -> 48.5 us  [collect(): theirs = lax.ppermute(grown, axis, [(d, d ^ reach) for d in range(ways)])]
    select_n x0 -> x2, other arithmetic: none -> 7.51 us  [collect(): grown = jnp.where(here & reach == 0, mine_first, theirs_first)]
    ppermute x0 -> x3, starting transfers between devices: none -> 6.24 us  [collect(): theirs = lax.ppermute(grown, axis, [(d, d ^ reach) for d in range(ways)])]
  transfers between devices with their start and end apart: 7 -> 9, of which waited for: 7 -> 8; matrix products, arithmetic and copies ran while one was open for 5% -> 3% of each run, Pallas kernels for 0% -> 0%
where the time goes in v1:
time: 466 us
  waiting for transfers between devices  347 us (74%)
  matrix products  44.7 us (10%)
  blocking collectives  22.7 us (5%)
  starting transfers between devices  14.8 us (3%)
  other arithmetic  13.7 us (3%)
  between operations  13.4 us (3%)
  local copies, waits for them, and re-layouts  8.5 us (2%)
    all_to_all x1, waiting for transfers between devices, shards(): lax.all_to_all(attended, 'tp', split_axis=0, concat_axis=1, tiled=True)  112 us
    reduce_scatter x1, waiting for transfers between devices, shards(): lax.psum_scatter(jnp.dot(hidden, down_weight[0], preferred_element_type=j...  68.5 us
    all_gather x1, waiting for transfers between devices, shards(): rows_in = lax.all_gather(row_block, 'tp', axis=0, tiled=True)  65 us
    ppermute x3, waiting for transfers between devices, collect(): theirs = lax.ppermute(grown, axis, [(d, d ^ reach) for d in range(ways)])  48.5 us
    all_gather x1, waiting for transfers between devices, shards(): value_piece = lax.all_gather(value_vectors, 'sp', axis=0, tiled=True)  26.9 us
    dot_general x1, matrix products, shards(): jnp.dot(hidden, down_weight[0], preferred_element_type=jnp.float32)  20.1 us
    all_gather x1, waiting for transfers between devices, shards(): key_piece = lax.all_gather(key_vectors, 'sp', axis=0, tiled=True)  16.5 us
    all_to_all x1, blocking collectives, shards(): lax.all_to_all(dispatch, 'sp', split_axis=0, concat_axis=0, tiled=True)  14.5 us
  transfers between devices with their start and end apart: 9, of which 8 were waited for; matrix products, arithmetic and copies ran while one was open for 3% of the time, Pallas kernels for 0%

profile of v1, /device:TPU:0, one launch (start us, length us, event | category | flops | bytes accessed | tf_op | source)
XLA Modules:
  0.0 465.7 jit_solution(7201131801019771721)
XLA Ops:
  7.0 2.5 collective-permute-done
  9.5 2.4 maximum_select_fusion.9
  11.9 3.0 collective-permute-start.1
  14.9 46.0 %collective-permute-done.1 = bf16[512,2048]{1,0:T(8,128)(2,1)} collective-permute-done((bf16[512,2048]{1,0:T(8,128)(2,1)S(1)}, bf16[512,2048]{1,0:T(8,128)(2,1)}, u32[]{:S(2)}, u32[]{:S(2)}) %collective-permute-start.1) | collective-permute-done | bytes 2097184 | tf_op jit(solution)/shard_map/ppermute | solution.py:14
  61.0 5.1 %maximum_select_fusion.2 = bf16[1024,2048]{1,0:T(8,128)(2,1)} fusion(bf16[512,2048]{1,0:T(8,128)(2,1)} %collective-permute-done.1, bf16[512,2048]{1,0:T(8,128)(2,1)S(1)} %maximum_select_fusion.9, pred[]{:T(512)S(6)} %eq.36), kind=kLoop, calls=%fused_computation.31 | loop fusion | flops 18874368 | bytes 8388609 | tf_op jit(solution)/shard_map/jit(_where)/select_n | solution.py:17
  66.1 2.8 collective-permute-start.2
  70.0 8.2 %all_gather.13 = f32[2048,4]{0,1:T(4,128)S(1)} all-gather(f32[512,4]{0,1:T(4,128)S(1)} %copy-done), channel_id=1, replica_groups=mesh['sp'=4,'tp'=8] {'sp'}, dimensions={0}, use_global_device_ids=true | all-gather | bytes 40960 | tf_op jit(solution)/shard_map/all_gather | solution.py:46
  78.2 16.5 %all-gather.4.cloned.1.call-done = bf16[2048,256]{1,0:T(8,128)(2,1)} async-done(((bf16[512,256]{1,0:T(8,128)(2,1)}), bf16[2048,256]{1,0:T(8,128)(2,1)}) %all-gather.4.cloned.1.call-update) | async-done | bytes 1048592 | tf_op jit(solution)/shard_map/all_gather | solution.py:81
  96.2 26.9 %all-gather.6.cloned.1.call-done = bf16[2048,256]{1,0:T(8,128)(2,1)} async-done(((bf16[512,256]{1,0:T(8,128)(2,1)}), bf16[2048,256]{1,0:T(8,128)(2,1)}) %all-gather.6.cloned.1.call-update) | async-done | bytes 1048592 | tf_op jit(solution)/shard_map/all_gather | solution.py:82
  124.7 11.5 %while.15 = (s32[]{:T(128)}, f32[4,512]{1,0:T(4,128)S(1)}, f32[4,512]{1,0:T(4,128)S(1)}, f32[4,512,64]{1,2,0:T(8,128)S(1)}, s32[2]{0:T(128)S(1)}, /*index=5*/s32...) while((s32[]{:T(128)}, f32[4,512]{1,0:T(4,128)S(1)}, ...), condition=%wide.region_5.6_spmd.clone, body=%wide.region_0.5_spmd.clone.sunk | while | flops 577508864 | bytes 31973756 | solution.py:101
  125.9 9.2 %conditional.3 = ((f32[4,512]{1,0:T(4,128)S(1)}, f32[4,512]{1,0:T(4,128)S(1)}, f32[4,512,64]{1,2,0:T(8,128)S(1)})) conditional(s32[]{:T(128)} %convert_element_type.83, (f32[4,512]{1,0:T(4,128)S(1)}, f32[4,512]{1,0:T(4,128)S(1)}, f32[4,512,64]{1,2,0:T(8,128)S(1)}) %tuple.42, (s32[]{:T(128)}, s32[]{:T(128)}, bf16[2,1024,256]{1,2,0:T(8,128)(2,1)S(1)}, ...), branch_computations={%region_1.1_spmd, %region_2.4_spmd} | conditional | flops 577508864 | bytes 31971410 | solution.py:99
  126.4 2.5 fusion.4
  129.0 2.9 fusion.3
  131.9 3.1 fusion.8
  137.6 4.6 all-to-all-start
  142.9 111.8 %all-to-all-done = bf16[8,64,256]{2,1,0:T(8,128)(2,1)S(1)} async-done(((bf16[8,64,256]{2,1,0:T(8,128)(2,1)}), bf16[8,64,256]{2,1,0:T(8,128)(2,1)S(1)}, u32[]{:S(2)}, u32[]{:S(2)}) %all-to-all-start) | async-done | bytes 262176 | tf_op jit(solution)/shard_map/all_to_all | solution.py:109
  254.8 7.3 %multiply_reduce_fusion.1 = (f32[64]{0:T(128)S(1)}, f32[64,2048]{1,0:T(8,128)S(1)}) fusion(bf16[64,2048]{1,0:T(8,128)(2,1)S(1)} %bitcast.68, bf16[1024,2048]{1,0:T(8,128)(2,1)} %collective-permute-done.2, bf16[1024,2048]{1,0:T(8,128)(2,1)} %maximum_select_fusion.2, pred[]{:T(512)S(6)} %eq.35, bf16[64,2048]{1,0:T(8,128)(2,1)S(1)} %copy-done.5), kind=kOutput, calls=%fused_computation.45 | convolution fusion | flops 575406016 | bytes 9437441 | tf_op jit(solution)/shard_map/dot_general | solution.py:110
  263.1 14.5 %all_to_all.29 = bf16[4,48,2048]{2,1,0:T(8,128)(2,1)} all-to-all(bf16[4,48,2048]{2,1,0:T(8,128)(2,1)S(1)} %bitcast.61), channel_id=1, replica_groups=mesh['sp'=4,'tp'=8] {'sp'}, dimensions={0} | all-to-all | bytes 1572864 | tf_op jit(solution)/shard_map/all_to_all | solution.py:131
  277.6 65.0 %all-gather.8.cloned.1.call-done = bf16[1536,2048]{1,0:T(8,128)(2,1)} async-done(((bf16[192,2048]{1,0:T(8,128)(2,1)}), bf16[1536,2048]{1,0:T(8,128)(2,1)}) %all-gather.8.cloned.1.call-update) | async-done | bytes 6291472 | tf_op jit(solution)/shard_map/all_gather | solution.py:133
  342.6 11.3 %fusion.25 = f32[1536,896]{1,0:T(8,128)} fusion(bf16[1536,2048]{1,0:T(8,128)(2,1)} %all-gather.8.cloned.1.call-done, bf16[1,2048,896]{2,1,0:T(8,128)(2,1)} %param.23), kind=kOutput, calls=%fused_computation.34 | convolution fusion | flops 5637144576 | bytes 15466496 | tf_op jit(solution)/shard_map/dot_general | solution.py:134
  353.9 20.1 %convolution_convert_fusion = bf16[1536,2048]{1,0:T(8,128)(2,1)} fusion(bf16[1,896,2048]{2,1,0:T(8,128)(2,1)} %param.25, f32[1536,896]{1,0:T(8,128)} %fusion.25, bf16[1536,2048]{1,0:T(8,128)(2,1)} %all-gather.8.cloned.1.call-done, bf16[1,2048,896]{2,1,0:T(8,128)(2,1)} %param.24), kind=kOutput, calls=%fused_computation.29 | convolution fusion | flops 11285692416 | bytes 25427968 | tf_op jit(solution)/shard_map/dot_general | solution.py:138
  374.0 68.5 %reduce-scatter.2.cloned.1.call-done = bf16[192,2048]{1,0:T(8,128)(2,1)} async-done(((bf16[1536,2048]{1,0:T(8,128)(2,1)}), bf16[192,2048]{1,0:T(8,128)(2,1)}) %reduce-scatter.2.cloned.1.call-update) | async-done | bytes 786448 | tf_op jit(solution)/shard_map/reduce_scatter | solution.py:137
  442.6 3.6 all-to-all-start.2
  446.6 8.7 %all-to-all-done.2 = bf16[4,48,2048]{2,1,0:T(8,128)(2,1)S(1)} async-done(((bf16[4,48,2048]{2,1,0:T(8,128)(2,1)}), bf16[4,48,2048]{2,1,0:T(8,128)(2,1)S(1)}, u32[]{:S(2)}, u32[]{:S(2)}) %all-to-all-start.2) | async-done | bytes 786464 | tf_op jit(solution)/shard_map/all_to_all | solution.py:144
  (67 shorter events, 13.7 us)
Async XLA Ops:
  6.5 88.2 %all-gather.4.cloned.1.call-start = ((), (), s32[]{:S(2)}) async-start(), calls=%async_computation.4 | async-start | bytes 1310720 | tf_op jit(solution)/shard_map/all_gather | solution.py:81
  6.5 3.0 collective-permute-start
  7.0 62.6 %copy-start.1 = (bf16[512,256]{1,0:T(8,128)(2,1)S(1)}, bf16[512,256]{1,0:T(8,128)(2,1)}, u32[]{:S(2)}) copy-start(bf16[512,256]{1,0:T(8,128)(2,1)} %param.17) | copy-start | bytes 786436
  7.0 62.7 %copy-start.3 = (s32[64,2]{0,1:T(2,128)S(1)}, s32[64,2]{0,1:T(2,128)}, u32[]{:S(2)}) copy-start(s32[64,2]{0,1:T(2,128)} %param.26) | copy-start | bytes 1540
  7.0 63.0 %copy-start = (f32[512,4]{0,1:T(4,128)S(1)}, f32[512,4]{0,1:T(4,128)}, u32[]{:S(2)}) copy-start(f32[512,4]{0,1:T(4,128)} %param.20) | copy-start | bytes 24580
  11.9 49.0 %collective-permute-start.1 = (bf16[512,2048]{1,0:T(8,128)(2,1)S(1)}, bf16[512,2048]{1,0:T(8,128)(2,1)}, u32[]{:S(2)}, u32[]{:S(2)}) collective-permute-start(bf16[512,2048]{1,0:T(8,128)(2,1)S(1)} %maximum_select_fusion.9), channel_id=1, source_target_pairs={{0,2},{1,3},{2,0},{3,1},{4,6},{5,7},{6,4},{7,5},{8,10},{9,11},{10,... | collective-permute-start | bytes 6291464 | tf_op jit(solution)/shard_map/ppermute | solution.py:14
  66.1 188.7 %collective-permute-start.2 = (bf16[1024,2048]{1,0:T(8,128)(2,1)}, bf16[1024,2048]{1,0:T(8,128)(2,1)}, u32[]{:S(2)}, u32[]{:S(2)}) collective-permute-start(bf16[1024,2048]{1,0:T(8,128)(2,1)} %maximum_select_fusion.2), channel_id=1, source_target_pairs={{0,4},{1,5},{2,6},{3,7},{4,0},{5,1},{6,2},{7,3},{8,12},{9,13},{10,... | collective-permute-start | bytes 12582920 | tf_op jit(solution)/shard_map/ppermute | solution.py:14
  68.9 54.2 %all-gather.6.cloned.1.call-start = ((), (), s32[]{:S(2)}) async-start(), calls=%async_computation.5 | async-start | bytes 1310720 | tf_op jit(solution)/shard_map/all_gather | solution.py:82
  124.7 130.1 %copy-start.5 = (bf16[64,2048]{1,0:T(8,128)(2,1)S(1)}, bf16[64,2048]{1,0:T(8,128)(2,1)}, u32[]{:S(2)}) copy-start(bf16[64,2048]{1,0:T(8,128)(2,1)} %param.16) | copy-start | bytes 786436
  137.6 117.1 %all-to-all-start = ((bf16[8,64,256]{2,1,0:T(8,128)(2,1)}), bf16[8,64,256]{2,1,0:T(8,128)(2,1)S(1)}, u32[]{:S(2)}, u32[]{:S(2)}) async-start(bf16[8,64,256]{2,1,0:T(8,128)(2,1)} %copy.30), calls=%async_computation | async-start | bytes 524288 | tf_op jit(solution)/shard_map/all_to_all | solution.py:109
  142.2 200.3 %all-gather.8.cloned.1.call-start = ((), (), s32[]{:S(2)}) async-start(), calls=%async_computation.6 | async-start | bytes 7077888 | tf_op jit(solution)/shard_map/all_gather | solution.py:133
  254.8 7.3 %copy-start.2 = (f32[2048]{0:T(1024)S(1)}, f32[2048]{0:T(1024)}, u32[]{:S(2)}) copy-start(f32[2048]{0:T(1024)} %param.22) | copy-start | bytes 24580
  277.6 165.0 %reduce-scatter.2.cloned.1.call-start = ((), (), s32[]{:S(2)}) async-start(), calls=%async_computation.7 | async-start | bytes 7077888 | tf_op jit(solution)/shard_map/reduce_scatter | solution.py:137
  374.0 72.4 %copy-start.4 = (f32[64,2]{0,1:T(2,128)S(1)}, f32[64,2]{0,1:T(2,128)}, u32[]{:S(2)}) copy-start(f32[64,2]{0,1:T(2,128)} %param.27) | copy-start | bytes 1540
  442.6 12.7 %all-to-all-start.2 = ((bf16[4,48,2048]{2,1,0:T(8,128)(2,1)}), bf16[4,48,2048]{2,1,0:T(8,128)(2,1)S(1)}, u32[]{:S(2)}, u32[]{:S(2)}) async-start(bf16[4,48,2048]{2,1,0:T(8,128)(2,1)} %bitcast.65), calls=%async_computation.3 | async-start | bytes 1572864 | tf_op jit(solution)/shard_map/all_to_all | solution.py:144
Sparse Core Ops, SparseCore 0:
  69.0 25.7 all-gather.3
  96.6 26.4 all-gather.5
  277.7 64.8 all-gather.7
  374.1 68.3 reduce-scatter.1
